TPU v7x, 256 devices: a 4x2x16 block of a 4x16x16 slice. The times are simulated.
256 devices in a mesh: grp: 2 (over y), sp: 32 (over z, core), tp: 4 (over x).
Axes of the slice: x: 4, y: 2, z: 16, core: 2. Of those that a mesh axis runs over, the one named last changes fastest.
The devices are a block of a 4x16x16 slice.
Arguments:
- gate_in: bfloat16 [32768, 1536], P(('grp', 'sp'), 'tp'), parts along dimension 0, may hold values from -6 to 6
- mult_in: bfloat16 [32768, 1536], P(('grp', 'sp'), 'tp'), parts along dimension 0, may hold values from -6 to 6
- value_in: bfloat16 [32768, 1536], P(('grp', 'sp'), 'tp'), parts along dimension 0, may hold values from -6 to 6
- doc_ids: int32 [32768], P(('grp', 'sp')), parts along dimension 0, may hold values from 0 to 15, never falling along the last dimension, each value on 1 to 1536 neighbouring positions
- conv_taps: bfloat16 [3, 1536], P(None, 'tp'), may hold values from -3 to 3
- out_proj: bfloat16 [1536, 2048], P('tp'), may hold values from -0.15625 to 0.15625
- resid: bfloat16 [32768, 2048], P(('grp', 'sp', 'tp')), parts along dimension 0, may hold values from -6 to 6
- norm1_gain: float32 [2048], replicated, may hold values from 0.1 to 1.9
- norm1_bias: float32 [2048], replicated, may hold values from -1.5 to 1.5
- expert_ids: int32 [32768, 2], P(('grp', 'sp', 'tp')), parts along dimension 0, may hold values from 0 to 31, all different within a row; in each aligned block of 128 rows (0 to 127, 128 to 255, ...) at most 10 rows name the same one
- expert_wts: float32 [32768, 2], P(('grp', 'sp', 'tp')), parts along dimension 0, may hold values from 0.1 to 1
- w_gate: bfloat16 [32, 2048, 3072], P('sp', None, 'tp'), may hold values from -0.125 to 0.125
- w_up: bfloat16 [32, 2048, 3072], P('sp', None, 'tp'), may hold values from -0.125 to 0.125
- w_down: bfloat16 [32, 3072, 2048], P('sp', 'tp'), may hold values from -0.21582031 to 0.21582031
- norm2_gain: float32 [2048], replicated, may hold values from 0.1 to 1.9
- norm2_bias: float32 [2048], replicated, may hold values from -1.5 to 1.5
Outputs:
- result: bfloat16 [32768, 2048], P(('grp', 'sp', 'tp')), parts along dimension 0
There are 2 independent parts, one for each index of `grp`. A program takes and returns all parts, laid end to end along the dimension named above; an argument that names none is the same for every part. Nothing has to cross between parts.
Inputs may be any that keep to these rules, and one draw needn't show every extreme that they name: `doc_ids`: never falling along the sequence; each document has 1 to 1536 positions and one has exactly 1536. `expert_ids`: each row names 2 different experts. Among the rows of one device no expert is named more than 10 times, and in some device's rows some expert is named exactly 10 times.
All inputs are finite; a program needn't handle non-finite values.
Results may differ from a plain program's by a relative error of at most 0.0095.
Values may be sent and summed in bfloat16 or wider, within the bound.
No kernel may reach another device: no remote copies, remote signals or barrier semaphores. Data moves between devices by JAX's collectives and lax.ppermute only.
A program may use at most 128 MiB of HBM per device.

v0:
```python
import jax
import jax.numpy as jnp
from jax import lax
from jax.sharding import Mesh
from jax.sharding import PartitionSpec as P

SP = ("sp_0", "sp_1")
GRP_SP = ("grp", "sp_0", "sp_1")
GRP_SP_TP = ("grp", "sp_0", "sp_1", "tp")
SUBLANES = 8
residual_scale = 2.0**0.5
norm_eps = 1e-05


def next_in_sequence(x):
    length = lax.axis_size(SP)
    return lax.ppermute(x, SP, [(i, i + 1) for i in range(length - 1)])


def swapped(x):
    return lax.ppermute(x, "sp_1", [(0, 1), (1, 0)])


def layer_norm(pre, gain, bias):
    center = pre - jnp.mean(pre, axis=-1, keepdims=True)
    spread = jnp.mean(center * center, axis=-1, keepdims=True)
    return center * lax.rsqrt(spread + norm_eps) * gain + bias


def dot(a, b):
    return jnp.dot(a, b, preferred_element_type=jnp.float32)


def chunk_slots(capacity, cores):
    width = SUBLANES // cores
    rest = capacity % width
    sizes = ([rest] if rest else []) + [width] * (capacity // width)
    starts = [sum(sizes[:i]) for i in range(len(sizes))]
    return list(zip(starts, sizes))


def shards(
    gate_in,
    mult_in,
    value_in,
    doc_ids,
    conv_taps,
    out_proj,
    resid,
    norm1_gain,
    norm1_bias,
    expert_ids,
    expert_wts,
    w_gate,
    w_up,
    w_down,
    norm2_gain,
    norm2_bias,
):
    n_tp = lax.axis_size("tp")
    chips = lax.axis_size("sp_0")
    cores = lax.axis_size("sp_1")
    experts = chips * cores
    tok_count, top_count = expert_ids.shape
    width = out_proj.shape[1]
    capacity = 5 * tok_count * top_count // (4 * experts)
    tap_weights = conv_taps.astype(jnp.float32)
    taps = tap_weights.shape[0]
    product = mult_in.astype(jnp.float32) * value_in.astype(jnp.float32)
    docs = doc_ids.astype(jnp.float32)
    row_count, channels = product.shape
    tail_docs = jnp.broadcast_to(docs[row_count - taps + 1 :, None], (taps - 1, channels))
    prev = next_in_sequence(jnp.concatenate([product[row_count - taps + 1 :], tail_docs], axis=0))
    prev_rows, prev_docs = (prev[: taps - 1], prev[taps - 1 :, 0])
    meta = jnp.concatenate([expert_ids.astype(jnp.float32).T, expert_wts.T], axis=0)
    metas = jnp.stack([meta, swapped(meta)])
    ext_rows = jnp.concatenate([prev_rows, product], axis=0)
    ext_docs = jnp.concatenate([prev_docs, docs], axis=0)
    filtered = jnp.zeros_like(product)
    for tap_index in range(taps):
        shifted = ext_rows[tap_index : tap_index + row_count]
        same_doc = (ext_docs[tap_index : tap_index + row_count] == docs)[:, None]
        filtered = filtered + tap_weights[tap_index] * jnp.where(same_doc, shifted, 0.0)
    mixed_heads = (gate_in.astype(jnp.float32) * filtered).astype(jnp.bfloat16)
    partial = dot(mixed_heads, out_proj).astype(jnp.bfloat16)
    partials = lax.all_to_all(
        partial.reshape(n_tp, row_count // n_tp, width), "tp", 0, 0, tiled=True
    )
    mixed = jnp.sum(partials.astype(jnp.float32), axis=0)
    hidden_one = layer_norm(
        residual_scale * resid.astype(jnp.float32) + mixed, norm1_gain, norm1_bias
    ).astype(jnp.bfloat16)
    hidden_both = jnp.concatenate([hidden_one, swapped(hidden_one)], axis=0)
    ids, wts = (metas[:, :top_count], metas[:, top_count:])
    numbers = (jnp.arange(chips) * cores + lax.axis_index("sp_1")).astype(jnp.float32)
    named = ids[:, :, None, :] == numbers[None, None, :, None]
    chosen = jnp.any(named, axis=1)
    weight = jnp.sum(jnp.where(named, wts[:, :, None, :], 0.0), axis=1)
    before = (jnp.arange(tok_count)[:, None] < jnp.arange(tok_count)[None, :]).astype(jnp.bfloat16)
    earlier = dot(chosen.astype(jnp.bfloat16), before)
    slot_of = jnp.where(chosen, earlier, -1.0)

    def selected(start, size, values):
        slots = (start + jnp.arange(size)).astype(jnp.float32)
        hit = slot_of.transpose(1, 0, 2)[:, :, None, None, :] == slots[None, None, :, None, None]
        same = jnp.arange(cores)[:, None] == jnp.arange(cores)[None, :]
        hit = hit & same[None, :, None, :, None]
        picked = jnp.where(hit, values.transpose(1, 0, 2)[:, :, None, None, :], 0.0)
        return picked.reshape(chips * cores * size, cores * tok_count)

    chunks = chunk_slots(capacity, cores)
    ones = jnp.ones_like(weight)
    packed = [
        dot(selected(start, size, ones).astype(jnp.bfloat16), hidden_both)
        .astype(jnp.bfloat16)
        .reshape(chips, cores * size, width)
        for start, size in chunks
    ]
    gathered = []
    for i in range(len(chunks)):
        moved = lax.all_to_all(packed[i], "sp_0", 0, 0, tiled=True)
        rest = tuple(packed[i + 1 :])
        moved, rest = lax.optimization_barrier((moved, rest))
        packed[i + 1 :] = list(rest)
        gathered.append(lax.all_gather(moved.reshape(-1, width), "tp", axis=0, tiled=True))
    scattered = []
    for rows_in in gathered:
        gate_act = dot(rows_in, w_gate[0])
        up_act = dot(rows_in, w_up[0])
        hid = (jax.nn.silu(gate_act) * up_act).astype(jnp.bfloat16)
        piece = dot(hid, w_down[0]).astype(jnp.bfloat16)
        scattered.append(lax.psum_scatter(piece, "tp", scatter_dimension=0, tiled=True))
    total = jnp.zeros((cores * tok_count, width), jnp.float32)
    for i, (start, size) in enumerate(chunks):
        ready = scattered[i].reshape(chips, cores * size, width)
        back = lax.all_to_all(ready, "sp_0", 0, 0, tiled=True).reshape(-1, width)
        factor = selected(start, size, weight)
        high = factor.astype(jnp.bfloat16)
        low = (factor - high.astype(jnp.float32)).astype(jnp.bfloat16)
        total = total + dot(high.T, back) + dot(low.T, back)
    moe = total[:tok_count] + swapped(total[tok_count:])
    return layer_norm(
        residual_scale * hidden_one.astype(jnp.float32) + moe, norm2_gain, norm2_bias
    ).astype(jnp.bfloat16)


def solution(mesh):
    torus = Mesh(
        mesh.devices.reshape(mesh.shape["grp"], -1, 2, mesh.shape["tp"]),
        ("grp", "sp_0", "sp_1", "tp"),
    )
    in_specs = (
        P(GRP_SP, "tp"),
        P(GRP_SP, "tp"),
        P(GRP_SP, "tp"),
        P(GRP_SP),
        P(None, "tp"),
        P("tp", None),
        P(GRP_SP_TP, None),
        P(),
        P(),
        P(GRP_SP_TP, None),
        P(GRP_SP_TP, None),
        P(SP, None, "tp"),
        P(SP, None, "tp"),
        P(SP, "tp", None),
        P(),
        P(),
    )
    out_specs = P(GRP_SP_TP, None)
    return jax.shard_map(
        shards, mesh=torus, in_specs=in_specs, out_specs=out_specs, check_vma=False
    )
```

profile of v0, /device:TPU:33, one launch (start us, length us, event | category | flops | bytes accessed | tf_op | source)
XLA Modules:
  0.0 383.8 jit_solution(6780999300419874182)
XLA Ops:
  6.6 0.8 convert_element_type.245
  7.5 1.2 convert_multiply_fusion
  8.9 5.7 %collective-permute-start = (f32[4,384]{1,0:T(4,128)S(1)}, f32[4,384]{1,0:T(4,128)S(1)}, u32[]{:S(2)}, u32[]{:S(2)}) collective-permute-start(f32[4,384]{1,0:T(4,128)S(1)} %pad_maximum_fusion.5), channel_id=1, source_target_pairs={{0,4},{4,8},{8,12},{12,16},{16,20},{20,24},{24,28},{28,32},{32,36}... | collective-permute-start | bytes 18440 | tf_op jit(solution)/shard_map/ppermute | solution.py:17
  15.3 15.9 %collective-permute-done = f32[4,384]{1,0:T(4,128)S(1)} collective-permute-done((f32[4,384]{1,0:T(4,128)S(1)}, f32[4,384]{1,0:T(4,128)S(1)}, u32[]{:S(2)}, u32[]{:S(2)}) %collective-permute-start) | collective-permute-done | bytes 6176 | tf_op jit(solution)/shard_map/ppermute | solution.py:17
  31.4 0.8 slice_compare_fusion.1
  32.2 4.4 %convolution_convert_fusion = bf16[512,2048]{1,0:T(8,128)(2,1)} fusion(bf16[384,2048]{1,0:T(8,128)(2,1)} %param.21, f32[2,384]{1,0:T(2,128)S(1)} %slice.63, f32[512,384]{1,0:T(8,128)S(1)} %convert_multiply_fusion, bf16[512,384]{1,0:T(8,128)(2,1)} %param.16, f32[384]{0:T(512)S(1)} %get-tuple-element.16, f32[384]{0:T(512)S(1)} %get-tuple-element.17, ...), kind=kOutput, calls=%fused_computation.21 | convolution fusion | flops 808910848 | bytes 4858880 | tf_op jit(solution)/shard_map/dot_general | solution.py:31
  36.6 4.7 %all-to-all-start = ((bf16[4,128,2048]{2,1,0:T(8,128)(2,1)}), bf16[4,128,2048]{2,1,0:T(8,128)(2,1)}, u32[]{:S(2)}, u32[]{:S(2)}) async-start(bf16[4,128,2048]{2,1,0:T(8,128)(2,1)} %bitcast.127), calls=%async_computation | async-start | bytes 4194304 | tf_op jit(solution)/shard_map/all_to_all | solution.py:86
  41.6 1.0 collective-permute-done.1
  42.8 24.7 %all-to-all-done = bf16[4,128,2048]{2,1,0:T(8,128)(2,1)} async-done(((bf16[4,128,2048]{2,1,0:T(8,128)(2,1)}), bf16[4,128,2048]{2,1,0:T(8,128)(2,1)}, u32[]{:S(2)}, u32[]{:S(2)}) %all-to-all-start) | async-done | bytes 2097184 | tf_op jit(solution)/shard_map/all_to_all | solution.py:86
  67.5 2.1 convert_reduce_fusion
  70.7 1.1 collective-permute-start.2
  73.4 0.8 copy-done.21
  74.5 0.8 reshape.246
  75.3 6.6 %all-to-all-start.1 = ((bf16[16,4,2048]{2,1,0:T(4,128)(2,1)}), bf16[16,4,2048]{2,1,0:T(4,128)(2,1)S(1)}, u32[]{:S(2)}, u32[]{:S(2)}) async-start(bf16[16,4,2048]{2,1,0:T(4,128)(2,1)} %reshape.246), calls=%async_computation.1 | async-start | bytes 524288 | tf_op jit(solution)/shard_map/all_to_all | solution.py:121
  82.1 1.8 fusion.83
  83.8 2.3 fusion.31
  86.2 1.1 fusion.32
  87.3 8.4 %all-to-all-done.1 = bf16[16,4,2048]{2,1,0:T(4,128)(2,1)S(1)} async-done(((bf16[16,4,2048]{2,1,0:T(4,128)(2,1)}), bf16[16,4,2048]{2,1,0:T(4,128)(2,1)S(1)}, u32[]{:S(2)}, u32[]{:S(2)}) %all-to-all-start.1) | async-done | bytes 262176 | tf_op jit(solution)/shard_map/all_to_all | solution.py:121
  95.7 10.4 %all-to-all-start.3 = ((bf16[16,8,2048]{2,1,0:T(8,128)(2,1)}), bf16[16,8,2048]{2,1,0:T(8,128)(2,1)}, u32[]{:S(2)}, u32[]{:S(2)}) async-start(bf16[16,8,2048]{2,1,0:T(8,128)(2,1)} %fusion.31), calls=%async_computation.4 | async-start | bytes 1048576 | tf_op jit(solution)/shard_map/all_to_all | solution.py:121
  106.2 0.8 reshape.249
  107.1 21.9 %all-to-all-done.3 = bf16[16,8,2048]{2,1,0:T(8,128)(2,1)} async-done(((bf16[16,8,2048]{2,1,0:T(8,128)(2,1)}), bf16[16,8,2048]{2,1,0:T(8,128)(2,1)}, u32[]{:S(2)}, u32[]{:S(2)}) %all-to-all-start.3) | async-done | bytes 524320 | tf_op jit(solution)/shard_map/all_to_all | solution.py:121
  129.1 35.6 %all_to_all.35 = bf16[16,8,2048]{2,1,0:T(8,128)(2,1)} all-to-all(bf16[16,8,2048]{2,1,0:T(8,128)(2,1)} %fusion.32), channel_id=1, replica_groups=mesh['grp'=2,'sp_0'=16,'sp_1'=2,'tp'=4] {'sp_0'}, dimensions={0} | all-to-all | bytes 1048576 | tf_op jit(solution)/shard_map/all_to_all | solution.py:121
  164.9 4.1 %fusion.16 = f32[256,768]{1,0:T(8,128)} fusion(bf16[256,2048]{1,0:T(8,128)(2,1)} %all-gather.4.cloned.1.call-done, bf16[1,2048,768]{2,1,0:T(8,128)(2,1)} %param.27), kind=kOutput, calls=%fused_computation.17 | convolution fusion | flops 805306368 | bytes 4980736 | tf_op jit(solution)/shard_map/dot_general | solution.py:31
  169.0 5.6 %fusion.28 = bf16[256,2048]{1,0:T(8,128)(2,1)} fusion(bf16[1,768,2048]{2,1,0:T(8,128)(2,1)S(1)} %copy-done, bf16[256,2048]{1,0:T(8,128)(2,1)} %all-gather.4.cloned.1.call-done, bf16[1,2048,768]{2,1,0:T(8,128)(2,1)} %param.28, f32[256,768]{1,0:T(8,128)} %fusion.16), kind=kOutput, calls=%fused_computation.27 | convolution fusion | flops 1612316672 | bytes 9175040 | tf_op jit(solution)/shard_map/dot_general | solution.py:31
  174.9 3.0 all-gather.6.cloned.1.call-done
  177.9 5.5 %fusion.14 = f32[512,768]{1,0:T(8,128)} fusion(bf16[512,2048]{1,0:T(8,128)(2,1)} %all-gather.6.cloned.1.call-done, bf16[1,2048,768]{2,1,0:T(8,128)(2,1)} %param.27), kind=kOutput, calls=%fused_computation.15 | convolution fusion | flops 1610612736 | bytes 6815744 | tf_op jit(solution)/shard_map/dot_general | solution.py:31
  183.3 8.2 %fusion.18 = bf16[512,2048]{1,0:T(8,128)(2,1)} fusion(bf16[1,768,2048]{2,1,0:T(8,128)(2,1)S(1)} %copy-done, f32[512,768]{1,0:T(8,128)} %fusion.14, bf16[512,2048]{1,0:T(8,128)(2,1)} %all-gather.6.cloned.1.call-done, bf16[1,2048,768]{2,1,0:T(8,128)(2,1)} %param.28), kind=kOutput, calls=%fused_computation.19 | convolution fusion | flops 3224633344 | bytes 12058624 | tf_op jit(solution)/shard_map/dot_general | solution.py:31
  191.7 24.9 %all-gather.8.cloned.1.call-done = bf16[512,2048]{1,0:T(8,128)(2,1)} async-done(((bf16[128,2048]{1,0:T(8,128)(2,1)}), bf16[512,2048]{1,0:T(8,128)(2,1)}) %all-gather.8.cloned.1.call-update) | async-done | bytes 2097168 | tf_op jit(solution)/shard_map/all_gather | solution.py:125
  216.7 5.5 %fusion.12 = f32[512,768]{1,0:T(8,128)} fusion(bf16[512,2048]{1,0:T(8,128)(2,1)} %all-gather.8.cloned.1.call-done, bf16[1,2048,768]{2,1,0:T(8,128)(2,1)} %param.27), kind=kOutput, calls=%fused_computation.13 | convolution fusion | flops 1610612736 | bytes 6815744 | tf_op jit(solution)/shard_map/dot_general | solution.py:31
  222.1 8.3 %fusion.21 = bf16[512,2048]{1,0:T(8,128)(2,1)} fusion(bf16[1,768,2048]{2,1,0:T(8,128)(2,1)S(1)} %copy-done, f32[512,768]{1,0:T(8,128)} %fusion.12, bf16[512,2048]{1,0:T(8,128)(2,1)} %all-gather.8.cloned.1.call-done, bf16[1,2048,768]{2,1,0:T(8,128)(2,1)} %param.28), kind=kOutput, calls=%fused_computation.20 | convolution fusion | flops 3224633344 | bytes 12058624 | tf_op jit(solution)/shard_map/dot_general | solution.py:31
  230.5 17.2 %reduce-scatter.4.cloned.1.call-done = bf16[64,2048]{1,0:T(8,128)(2,1)} async-done(((bf16[256,2048]{1,0:T(8,128)(2,1)}), bf16[64,2048]{1,0:T(8,128)(2,1)}) %reduce-scatter.4.cloned.1.call-update) | async-done | bytes 262160 | tf_op jit(solution)/shard_map/reduce_scatter | solution.py:132
  247.7 1.1 reshape.250
  248.7 24.5 %all_to_all.36 = bf16[16,4,2048]{2,1,0:T(4,128)(2,1)} all-to-all(bf16[16,4,2048]{2,1,0:T(4,128)(2,1)S(1)} %reshape.250), channel_id=1, replica_groups=mesh['grp'=2,'sp_0'=16,'sp_1'=2,'tp'=4] {'sp_0'}, dimensions={0} | all-to-all | bytes 524288 | tf_op jit(solution)/shard_map/all_to_all | solution.py:136
  273.3 13.8 %reduce-scatter.6.cloned.1.call-done = bf16[128,2048]{1,0:T(8,128)(2,1)} async-done(((bf16[512,2048]{1,0:T(8,128)(2,1)}), bf16[128,2048]{1,0:T(8,128)(2,1)}) %reduce-scatter.6.cloned.1.call-update) | async-done | bytes 524304 | tf_op jit(solution)/shard_map/reduce_scatter | solution.py:132
  287.0 35.0 %all_to_all.37 = bf16[16,8,2048]{2,1,0:T(8,128)(2,1)} all-to-all(bf16[16,8,2048]{2,1,0:T(8,128)(2,1)} %bitcast.130), channel_id=1, replica_groups=mesh['grp'=2,'sp_0'=16,'sp_1'=2,'tp'=4] {'sp_0'}, dimensions={0} | all-to-all | bytes 1048576 | tf_op jit(solution)/shard_map/all_to_all | solution.py:136
  322.0 3.0 reduce-scatter.8.cloned.1.call-done
  325.0 12.1 %all-to-all-start.6 = ((bf16[16,8,2048]{2,1,0:T(8,128)(2,1)}), bf16[16,8,2048]{2,1,0:T(8,128)(2,1)}, u32[]{:S(2)}, u32[]{:S(2)}) async-start(bf16[16,8,2048]{2,1,0:T(8,128)(2,1)} %bitcast.129), calls=%async_computation.9 | async-start | bytes 1048576 | tf_op jit(solution)/shard_map/all_to_all | solution.py:136
  337.9 1.0 reshape.251
  338.9 2.6 fusion.109
  341.5 1.8 fusion.64
  343.3 1.8 fusion.66
  345.1 14.9 %all-to-all-done.6 = bf16[16,8,2048]{2,1,0:T(8,128)(2,1)} async-done(((bf16[16,8,2048]{2,1,0:T(8,128)(2,1)}), bf16[16,8,2048]{2,1,0:T(8,128)(2,1)}, u32[]{:S(2)}, u32[]{:S(2)}) %all-to-all-start.6) | async-done | bytes 524320 | tf_op jit(solution)/shard_map/all_to_all | solution.py:136
  360.0 1.6 fusion.60
  361.7 1.5 fusion.62
  363.2 2.5 fusion.27
  365.8 7.2 %collective-permute-start.3 = (f32[128,2048]{1,0:T(8,128)S(1)}, f32[128,2048]{1,0:T(8,128)S(1)}, u32[]{:S(2)}, u32[]{:S(2)}) collective-permute-start(f32[128,2048]{1,0:T(8,128)S(1)} %slice.71), channel_id=1, source_target_pairs={{0,4},{4,0},{1,5},{5,1},{2,6},{6,2},{3,7},{7,3},{8,12},{12,8},{9,1... | collective-permute-start | bytes 3145736 | tf_op jit(solution)/shard_map/ppermute | solution.py:21
  373.0 2.3 collective-permute-done.3
  375.9 1.0 add_convert_fusion
  (96 shorter events, 6.9 us)
Async XLA Ops:
  6.5 162.5 %copy-start = (bf16[1,768,2048]{2,1,0:T(8,128)(2,1)S(1)}, bf16[1,768,2048]{2,1,0:T(8,128)(2,1)}, u32[]{:S(2)}) copy-start(bf16[1,768,2048]{2,1,0:T(8,128)(2,1)} %param.29) | copy-start | bytes 9437188
  8.9 22.4 %collective-permute-start = (f32[4,384]{1,0:T(4,128)S(1)}, f32[4,384]{1,0:T(4,128)S(1)}, u32[]{:S(2)}, u32[]{:S(2)}) collective-permute-start(f32[4,384]{1,0:T(4,128)S(1)} %pad_maximum_fusion.5), channel_id=1, source_target_pairs={{0,4},{4,8},{8,12},{12,16},{16,20},{20,24},{24,28},{28,32},{32,36}... | collective-permute-start | bytes 18440 | tf_op jit(solution)/shard_map/ppermute | solution.py:17
  36.6 4.7 %copy-start.19 = (s32[128,2]{0,1:T(2,128)S(1)}, s32[128,2]{0,1:T(2,128)}, u32[]{:S(2)}) copy-start(s32[128,2]{0,1:T(2,128)} %param.25) | copy-start | bytes 3076
  36.6 4.7 %copy-start.20 = (f32[128,2]{0,1:T(2,128)S(1)}, f32[128,2]{0,1:T(2,128)}, u32[]{:S(2)}) copy-start(f32[128,2]{0,1:T(2,128)} %param.26) | copy-start | bytes 3076
  36.6 30.9 %all-to-all-start = ((bf16[4,128,2048]{2,1,0:T(8,128)(2,1)}), bf16[4,128,2048]{2,1,0:T(8,128)(2,1)}, u32[]{:S(2)}, u32[]{:S(2)}) async-start(bf16[4,128,2048]{2,1,0:T(8,128)(2,1)} %bitcast.127), calls=%async_computation | async-start | bytes 4194304 | tf_op jit(solution)/shard_map/all_to_all | solution.py:86
  41.3 1.3 collective-permute-start.1
  41.6 30.5 %copy-start.17 = (pred[2,2]{1,0:T(4,128)(4,1)}, pred[2,2]{1,0:T(4,128)(4,1)S(1)}, u32[]{:S(2)}) copy-start(pred[2,2]{1,0:T(4,128)(4,1)S(1)} %iota_compare_fusion.1) | copy-start | bytes 16
  67.5 2.2 copy-start.3
  69.7 0.7 copy-start.13
  69.7 0.7 copy-start.14
  70.7 2.7 copy-start.5
  70.7 2.7 collective-permute-start.2
  72.1 1.3 copy-start.10
  73.4 0.8 copy-start.21
  75.3 20.4 %all-to-all-start.1 = ((bf16[16,4,2048]{2,1,0:T(4,128)(2,1)}), bf16[16,4,2048]{2,1,0:T(4,128)(2,1)S(1)}, u32[]{:S(2)}, u32[]{:S(2)}) async-start(bf16[16,4,2048]{2,1,0:T(4,128)(2,1)} %reshape.246), calls=%async_computation.1 | async-start | bytes 524288 | tf_op jit(solution)/shard_map/all_to_all | solution.py:121
  81.9 4.3 %copy-start.6 = (bf16[128,2048]{1,0:T(8,128)(2,1)S(1)}, bf16[128,2048]{1,0:T(8,128)(2,1)}, u32[]{:S(2)}) copy-start(bf16[128,2048]{1,0:T(8,128)(2,1)} %copy-done.5) | copy-start | bytes 1572868
  81.9 4.2 %copy-start.22 = (bf16[128,2048]{1,0:T(8,128)(2,1)S(1)}, bf16[128,2048]{1,0:T(8,128)(2,1)}, u32[]{:S(2)}) copy-start(bf16[128,2048]{1,0:T(8,128)(2,1)} %copy-done.21) | copy-start | bytes 1572868
  95.7 33.3 %all-to-all-start.3 = ((bf16[16,8,2048]{2,1,0:T(8,128)(2,1)}), bf16[16,8,2048]{2,1,0:T(8,128)(2,1)}, u32[]{:S(2)}, u32[]{:S(2)}) async-start(bf16[16,8,2048]{2,1,0:T(8,128)(2,1)} %fusion.31), calls=%async_computation.4 | async-start | bytes 1048576 | tf_op jit(solution)/shard_map/all_to_all | solution.py:121
  106.2 58.7 %all-gather.4.cloned.1.call-start = ((), (), s32[]{:S(2)}) async-start(), calls=%async_computation.10 | async-start | bytes 1310720 | tf_op jit(solution)/shard_map/all_gather | solution.py:125
  107.1 70.8 %all-gather.6.cloned.1.call-start = ((), (), s32[]{:S(2)}) async-start(), calls=%async_computation.12 | async-start | bytes 2621440 | tf_op jit(solution)/shard_map/all_gather | solution.py:125
  129.1 87.6 %all-gather.8.cloned.1.call-start = ((), (), s32[]{:S(2)}) async-start(), calls=%async_computation.14 | async-start | bytes 2621440 | tf_op jit(solution)/shard_map/all_gather | solution.py:125
  164.8 82.9 %reduce-scatter.4.cloned.1.call-start = ((), (), s32[]{:S(2)}) async-start(), calls=%async_computation.11 | async-start | bytes 1310720 | tf_op jit(solution)/shard_map/reduce_scatter | solution.py:132
  174.7 112.3 %reduce-scatter.6.cloned.1.call-start = ((), (), s32[]{:S(2)}) async-start(), calls=%async_computation.13 | async-start | bytes 2621440 | tf_op jit(solution)/shard_map/reduce_scatter | solution.py:132
  191.7 133.4 %reduce-scatter.8.cloned.1.call-start = ((), (), s32[]{:S(2)}) async-start(), calls=%async_computation.15 | async-start | bytes 2621440 | tf_op jit(solution)/shard_map/reduce_scatter | solution.py:132
  273.3 63.9 %copy-start.11 = (pred[16,2,2,128]{3,2,1,0:T(4,128)(4,1)S(1)}, pred[16,2,2,128]{3,2,1,0:T(4,128)(4,1)}, u32[]{:S(2)}) copy-start(pred[16,2,2,128]{3,2,1,0:T(4,128)(4,1)} %copy-done.10) | copy-start | bytes 24580
  273.3 63.9 %copy-start.18 = (pred[2,2]{1,0:T(4,128)(4,1)S(1)}, pred[2,2]{1,0:T(4,128)(4,1)}, u32[]{:S(2)}) copy-start(pred[2,2]{1,0:T(4,128)(4,1)} %copy-done.17) | copy-start | bytes 16
  325.0 35.0 %all-to-all-start.6 = ((bf16[16,8,2048]{2,1,0:T(8,128)(2,1)}), bf16[16,8,2048]{2,1,0:T(8,128)(2,1)}, u32[]{:S(2)}, u32[]{:S(2)}) async-start(bf16[16,8,2048]{2,1,0:T(8,128)(2,1)} %bitcast.129), calls=%async_computation.9 | async-start | bytes 1048576 | tf_op jit(solution)/shard_map/all_to_all | solution.py:136
  338.9 2.6 copy-start.4
  338.9 2.6 copy-start.9
  338.9 4.4 %copy-start.8 = (bf16[16,2,4,2,128]{4,3,2,1,0:T(2,128)(2,1)S(1)}, bf16[16,2,4,2,128]{4,3,2,1,0:T(2,128)(2,1)}, u32[]{:S(2)}) copy-start(bf16[16,2,4,2,128]{4,3,2,1,0:T(2,128)(2,1)} %get-tuple-element.21) | copy-start | bytes 196612
  360.0 3.1 copy-start.1
  360.0 3.2 copy-start.2
  360.0 3.2 copy-start.12
  365.7 9.6 %copy-start.7 = (bf16[128,2048]{1,0:T(8,128)(2,1)S(1)}, bf16[128,2048]{1,0:T(8,128)(2,1)}, u32[]{:S(2)}) copy-start(bf16[128,2048]{1,0:T(8,128)(2,1)} %copy-done.5) | copy-start | bytes 1572868
  365.8 10.1 %copy-start.15 = (f32[2048]{0:T(1024)S(1)}, f32[2048]{0:T(1024)}, u32[]{:S(2)}) copy-start(f32[2048]{0:T(1024)} %param.31) | copy-start | bytes 24580
  365.8 10.1 %copy-start.16 = (f32[2048]{0:T(1024)S(1)}, f32[2048]{0:T(1024)}, u32[]{:S(2)}) copy-start(f32[2048]{0:T(1024)} %param.30) | copy-start | bytes 24580
  365.8 9.4 %collective-permute-start.3 = (f32[128,2048]{1,0:T(8,128)S(1)}, f32[128,2048]{1,0:T(8,128)S(1)}, u32[]{:S(2)}, u32[]{:S(2)}) collective-permute-start(f32[128,2048]{1,0:T(8,128)S(1)} %slice.71), channel_id=1, source_target_pairs={{0,4},{4,0},{1,5},{5,1},{2,6},{6,2},{3,7},{7,3},{8,12},{12,8},{9,1... | collective-permute-start | bytes 3145736 | tf_op jit(solution)/shard_map/ppermute | solution.py:21
Sparse Core Ops, SparseCore 0:
  108.8 27.9 all-gather.3
  138.7 39.1 all-gather.5
  179.7 36.8 all-gather.7
  219.1 28.5 reduce-scatter.3
  250.1 36.8 reduce-scatter.5
  289.4 35.5 reduce-scatter.7
where the time goes:
time: 385 us; the launch traced here: 384 us
  waiting for transfers between devices  152 us (39%)
  blocking collectives  95.1 us (25%)
  matrix products  57.3 us (15%)
  starting transfers between devices  48.7 us (13%)
  between operations  13.9 us (4%)
  other arithmetic  11.9 us (3%)
  local copies, waits for them, and re-layouts  5.08 us (1%)
    all_to_all x2, blocking collectives, shards(): back = lax.all_to_all(ready, 'sp_0', 0, 0, tiled=True).reshape(-1, width)  59.5 us
    dot_general x17, matrix products, dot(): return jnp.dot(a, b, preferred_element_type=jnp.float32)  57.3 us
    all_to_all x1, blocking collectives, shards(): moved = lax.all_to_all(packed[i], 'sp_0', 0, 0, tiled=True)  35.6 us
    reduce_scatter x3, waiting for transfers between devices, shards(): lax.psum_scatter(piece, 'tp', scatter_dimension=0, tiled=True)  34 us
    all_to_all x2, waiting for transfers between devices, shards(): moved = lax.all_to_all(packed[i], 'sp_0', 0, 0, tiled=True)  30.3 us
    all_gather x3, waiting for transfers between devices, shards(): lax.all_gather(moved.reshape(-1, width), 'tp', axis=0, tiled=True)  27.9 us
    all_to_all x1, waiting for transfers between devices, shards(): lax.all_to_all(partial.reshape(n_tp, row_count // n_tp, width), 'tp', 0,...  24.7 us
    all_to_all x2, starting transfers between devices, shards(): moved = lax.all_to_all(packed[i], 'sp_0', 0, 0, tiled=True)  17 us
  transfers between devices with their start and end apart: 14, of which 13 were waited for; matrix products, arithmetic and copies ran while one was open for 14% of the time, Pallas kernels for 0%

commit v1 on v0

--- a/solution.py
+++ b/solution.py
@@ -1,3 +1,4 @@
+import functools
 import jax
 import jax.numpy as jnp
 from jax import lax
@@ -10,6 +11,43 @@
 SUBLANES = 8
 residual_scale = 2.0**0.5
 norm_eps = 1e-05
+
+
+def meet_page_up(sheet, dim_at):
+    sheet = jnp.moveaxis(sheet, 0, dim_at)
+    out_arr = sheet.shape
+    return sheet.reshape(
+        *out_arr[:dim_at], out_arr[dim_at] * out_arr[dim_at + 1], *out_arr[dim_at + 2 :]
+    )
+
+
+def trails_form(unit, which_axis, out_dim):
+    devs = lax.axis_size(which_axis)
+    lanes = []
+    for h in tuple(range(devs)):
+        lanes.append((h, (h + 1) % devs))
+    pool = []
+    for pp, idx in lanes:
+        pool.append((idx, pp))
+    block_now, outcome_arr = ([], [])
+    for rr in [*range(devs - 1)]:
+        if rr % 2 == 0:
+            block_now.append(
+                lax.ppermute(block_now[-1] if block_now else unit, axis_name=which_axis, perm=lanes)
+            )
+        else:
+            outcome_arr.append(
+                lax.ppermute(outcome_arr[-1] if outcome_arr else unit, which_axis, perm=pool)
+            )
+    z2 = jnp.stack([*block_now[::-1], unit, *outcome_arr])
+    tmp = lax.axis_index(which_axis)
+    opened = len(block_now)
+    row_out = tmp - opened
+    z2 = z2[(jnp.arange(devs) - row_out) % devs]
+    return meet_page_up(z2, out_dim)
+
+
+divide_the_vector = functools.partial(trails_form, which_axis="tp", out_dim=0)
 
 
 def next_in_sequence(x):
@@ -122,7 +160,7 @@
         rest = tuple(packed[i + 1 :])
         moved, rest = lax.optimization_barrier((moved, rest))
         packed[i + 1 :] = list(rest)
-        gathered.append(lax.all_gather(moved.reshape(-1, width), "tp", axis=0, tiled=True))
+        gathered.append(divide_the_vector(moved.reshape(-1, width)))
     scattered = []
     for rows_in in gathered:
         gate_act = dot(rows_in, w_gate[0])

time: 385 us -> 364 us (0.945)
  waiting for transfers between devices: 152 us -> 114 us
  blocking collectives: 95.1 us -> 69.8 us
  starting transfers between devices: 48.7 us -> 71.5 us
  local copies, waits for them, and re-layouts: 5.08 us -> 16.2 us
  other arithmetic: 11.9 us -> 20.5 us
    all_to_all x1 -> x0, blocking collectives: 35.6 us -> none  [shards(): moved = lax.all_to_all(packed[i], 'sp_0', 0, 0, tiled=True)]
    reduce_scatter x3, waiting for transfers between devices: 34 us -> 0.02 us  [shards(): lax.psum_scatter(piece, 'tp', scatter_dimension=0, tiled=True)]
    ppermute x0 -> x9, waiting for transfers between devices: none -> 31.5 us  [the longest x6 31.5 us: trails_form(): lax.ppermute(block_now[-1] if block_now else unit, axis_name=which_axis,...]
    all_gather x3 -> x0, waiting for transfers between devices: 27.9 us -> none  [shards(): lax.all_gather(moved.reshape(-1, width), 'tp', axis=0, tiled=True)]
    all_to_all x2 -> x3, starting transfers between devices: 17 us -> 32.1 us  [shards(): moved = lax.all_to_all(packed[i], 'sp_0', 0, 0, tiled=True)]
    gather x0 -> x3, local copies, waits for them, and re-layouts: none -> 10.4 us  [trails_form(): z2 = z2[(jnp.arange(devs) - row_out) % devs]]
    all_to_all x2, blocking collectives: 59.5 us -> 69.8 us  [shards(): back = lax.all_to_all(ready, 'sp_0', 0, 0, tiled=True).reshape(-1, width)]
    ppermute x0 -> x9, starting transfers between devices: none -> 8.04 us  [the longest x3 7.04 us: trails_form(): lax.ppermute(outcome_arr[-1] if outcome_arr else unit, which_axis, perm=p...]
  transfers between devices with their start and end apart: 14 -> 21, of which waited for: 13 -> 12; matrix products, arithmetic and copies ran while one was open for 14% -> 20% of each run, Pallas kernels for 0% -> 0%
where the time goes in v1:
time: 364 us; the launch traced here: 363 us
  waiting for transfers between devices  114 us (31%)
  starting transfers between devices  71.5 us (20%)
  blocking collectives  69.8 us (19%)
  matrix products  57.4 us (16%)
  other arithmetic  20.5 us (6%)
  local copies, waits for them, and re-layouts  16.2 us (4%)
  between operations  13.6 us (4%)
    all_to_all x2, blocking collectives, shards(): back = lax.all_to_all(ready, 'sp_0', 0, 0, tiled=True).reshape(-1, width)  69.8 us
    dot_general x17, matrix products, dot(): return jnp.dot(a, b, preferred_element_type=jnp.float32)  57.4 us
    all_to_all x3, starting transfers between devices, shards(): moved = lax.all_to_all(packed[i], 'sp_0', 0, 0, tiled=True)  32.1 us
    ppermute x6, waiting for transfers between devices, trails_form(): lax.ppermute(block_now[-1] if block_now else unit, axis_name=which_axis,...  31.5 us
    all_to_all x1, waiting for transfers between devices, shards(): lax.all_to_all(partial.reshape(n_tp, row_count // n_tp, width), 'tp', 0,...  24.7 us
    all_to_all x3, waiting for transfers between devices, shards(): moved = lax.all_to_all(packed[i], 'sp_0', 0, 0, tiled=True)  22.5 us
    ppermute x1, waiting for transfers between devices, next_in_sequence(): return lax.ppermute(x, SP, [(i, i + 1) for i in range(length - 1)])  15.9 us
    all_to_all x1, waiting for transfers between devices, shards(): back = lax.all_to_all(ready, 'sp_0', 0, 0, tiled=True).reshape(-1, width)  15 us
  transfers between devices with their start and end apart: 21, of which 12 were waited for; matrix products, arithmetic and copies ran while one was open for 20% of the time, Pallas kernels for 0%

profile of v1, /device:TPU:33, one launch (start us, length us, event | category | flops | bytes accessed | tf_op | source)
XLA Modules:
  0.0 362.6 jit_solution(16732855878891076886)
XLA Ops:
  7.5 1.2 convert_multiply_fusion
  8.9 5.7 %collective-permute-start = (f32[4,384]{1,0:T(4,128)S(1)}, f32[4,384]{1,0:T(4,128)S(1)}, u32[]{:S(2)}, u32[]{:S(2)}) collective-permute-start(f32[4,384]{1,0:T(4,128)S(1)} %pad_maximum_fusion.8), channel_id=1, source_target_pairs={{0,4},{4,8},{8,12},{12,16},{16,20},{20,24},{24,28},{28,32},{32,36}... | collective-permute-start | bytes 18440 | tf_op jit(solution)/shard_map/ppermute | solution.py:55
  15.3 15.9 %collective-permute-done = f32[4,384]{1,0:T(4,128)S(1)} collective-permute-done((f32[4,384]{1,0:T(4,128)S(1)}, f32[4,384]{1,0:T(4,128)S(1)}, u32[]{:S(2)}, u32[]{:S(2)}) %collective-permute-start) | collective-permute-done | bytes 6176 | tf_op jit(solution)/shard_map/ppermute | solution.py:55
  32.2 4.4 %convolution_convert_fusion = bf16[512,2048]{1,0:T(8,128)(2,1)} fusion(bf16[384,2048]{1,0:T(8,128)(2,1)} %param.21, f32[2,384]{1,0:T(2,128)S(1)} %slice.69, f32[512,384]{1,0:T(8,128)S(1)} %convert_multiply_fusion, bf16[512,384]{1,0:T(8,128)(2,1)} %param.16, f32[384]{0:T(512)S(1)} %get-tuple-element.16, f32[384]{0:T(512)S(1)} %get-tuple-element.17, ...), kind=kOutput, calls=%fused_computation.24 | convolution fusion | flops 808910848 | bytes 4858880 | tf_op jit(solution)/shard_map/dot_general | solution.py:69
  36.6 4.7 %all-to-all-start = ((bf16[4,128,2048]{2,1,0:T(8,128)(2,1)}), bf16[4,128,2048]{2,1,0:T(8,128)(2,1)}, u32[]{:S(2)}, u32[]{:S(2)}) async-start(bf16[4,128,2048]{2,1,0:T(8,128)(2,1)} %bitcast.143), calls=%async_computation | async-start | bytes 4194304 | tf_op jit(solution)/shard_map/all_to_all | solution.py:124
  42.8 24.7 %all-to-all-done = bf16[4,128,2048]{2,1,0:T(8,128)(2,1)} async-done(((bf16[4,128,2048]{2,1,0:T(8,128)(2,1)}), bf16[4,128,2048]{2,1,0:T(8,128)(2,1)}, u32[]{:S(2)}, u32[]{:S(2)}) %all-to-all-start) | async-done | bytes 2097184 | tf_op jit(solution)/shard_map/all_to_all | solution.py:124
  67.5 2.1 convert_reduce_fusion
  70.7 1.1 collective-permute-start.2
  75.3 6.6 %all-to-all-start.1 = ((bf16[16,4,2048]{2,1,0:T(4,128)(2,1)}), bf16[16,4,2048]{2,1,0:T(4,128)(2,1)S(1)}, u32[]{:S(2)}, u32[]{:S(2)}) async-start(bf16[16,4,2048]{2,1,0:T(4,128)(2,1)} %reshape.304), calls=%async_computation.1 | async-start | bytes 524288 | tf_op jit(solution)/shard_map/all_to_all | solution.py:159
  82.0 1.8 fusion.83
  83.8 2.3 fusion.31
  86.1 1.1 fusion.32
  87.2 8.5 %all-to-all-done.1 = bf16[16,4,2048]{2,1,0:T(4,128)(2,1)S(1)} async-done(((bf16[16,4,2048]{2,1,0:T(4,128)(2,1)}), bf16[16,4,2048]{2,1,0:T(4,128)(2,1)S(1)}, u32[]{:S(2)}, u32[]{:S(2)}) %all-to-all-start.1) | async-done | bytes 262176 | tf_op jit(solution)/shard_map/all_to_all | solution.py:159
  95.7 10.4 %all-to-all-start.3 = ((bf16[16,8,2048]{2,1,0:T(8,128)(2,1)}), bf16[16,8,2048]{2,1,0:T(8,128)(2,1)}, u32[]{:S(2)}, u32[]{:S(2)}) async-start(bf16[16,8,2048]{2,1,0:T(8,128)(2,1)} %fusion.31), calls=%async_computation.4 | async-start | bytes 1048576 | tf_op jit(solution)/shard_map/all_to_all | solution.py:159
  107.4 2.2 collective-permute-start.5
  109.6 5.8 %collective-permute-done.3 = bf16[64,2048]{1,0:T(8,128)(2,1)} collective-permute-done((bf16[64,2048]{1,0:T(8,128)(2,1)}, bf16[64,2048]{1,0:T(8,128)(2,1)}, u32[]{:S(2)}, u32[]{:S(2)}) %collective-permute-start.3) | collective-permute-done | bytes 262176 | tf_op jit(solution)/shard_map/ppermute | solution.py:36
  116.8 12.1 %all-to-all-done.3 = bf16[16,8,2048]{2,1,0:T(8,128)(2,1)} async-done(((bf16[16,8,2048]{2,1,0:T(8,128)(2,1)}), bf16[16,8,2048]{2,1,0:T(8,128)(2,1)}, u32[]{:S(2)}, u32[]{:S(2)}) %all-to-all-start.3) | async-done | bytes 524320 | tf_op jit(solution)/shard_map/all_to_all | solution.py:159
  129.5 2.3 pad_maximum_fusion.3
  131.8 2.9 gather_fusion
  134.7 4.1 %fusion.16 = f32[256,768]{1,0:T(8,128)} fusion(bf16[256,2048]{1,0:T(8,128)(2,1)} %bitcast.148, bf16[1,2048,768]{2,1,0:T(8,128)(2,1)} %param.27), kind=kOutput, calls=%fused_computation.20 | convolution fusion | flops 805306368 | bytes 4980736 | tf_op jit(solution)/shard_map/dot_general | solution.py:69
  138.8 2.2 collective-permute-start.8
  141.0 5.6 %fusion.28 = bf16[256,2048]{1,0:T(8,128)(2,1)} fusion(bf16[1,768,2048]{2,1,0:T(8,128)(2,1)S(1)} %copy-done, bf16[256,2048]{1,0:T(8,128)(2,1)} %bitcast.149, bf16[1,2048,768]{2,1,0:T(8,128)(2,1)} %param.28, f32[256,768]{1,0:T(8,128)} %fusion.16), kind=kOutput, calls=%fused_computation.30 | convolution fusion | flops 1612316672 | bytes 9175040 | tf_op jit(solution)/shard_map/dot_general | solution.py:69
  146.6 15.2 %all-to-all-start.5 = ((bf16[16,8,2048]{2,1,0:T(8,128)(2,1)}), bf16[16,8,2048]{2,1,0:T(8,128)(2,1)}, u32[]{:S(2)}, u32[]{:S(2)}) async-start(bf16[16,8,2048]{2,1,0:T(8,128)(2,1)} %fusion.32), calls=%async_computation.7 | async-start | bytes 1048576 | tf_op jit(solution)/shard_map/all_to_all | solution.py:159
  161.9 3.1 pad_maximum_fusion
  165.0 3.7 %gather_fusion.1 = bf16[4,128,2048]{2,1,0:T(8,128)(2,1)} fusion(bf16[4,128,2048]{2,1,0:T(8,128)(2,1)} %pad_maximum_fusion, s32[1024]{0:T(1024)} %pad_clamp_fusion), kind=kCustom, calls=%fused_computation.1 | custom fusion | bytes 4194320 | tf_op jit(solution)/shard_map/gather | solution.py:46
  168.7 5.5 %fusion.14 = f32[512,768]{1,0:T(8,128)} fusion(bf16[512,2048]{1,0:T(8,128)(2,1)} %bitcast.146, bf16[1,2048,768]{2,1,0:T(8,128)(2,1)} %param.27), kind=kOutput, calls=%fused_computation.18 | convolution fusion | flops 1610612736 | bytes 6815744 | tf_op jit(solution)/shard_map/dot_general | solution.py:69
  174.2 8.3 %fusion.18 = bf16[512,2048]{1,0:T(8,128)(2,1)} fusion(bf16[1,768,2048]{2,1,0:T(8,128)(2,1)S(1)} %copy-done, f32[512,768]{1,0:T(8,128)} %fusion.14, bf16[512,2048]{1,0:T(8,128)(2,1)} %bitcast.147, bf16[1,2048,768]{2,1,0:T(8,128)(2,1)} %param.28), kind=kOutput, calls=%fused_computation.22 | convolution fusion | flops 3224633344 | bytes 12058624 | tf_op jit(solution)/shard_map/dot_general | solution.py:69
  182.6 1.9 all-to-all-done.5
  184.5 2.7 collective-permute-start.11
  187.2 6.8 %collective-permute-done.9 = bf16[128,2048]{1,0:T(8,128)(2,1)S(1)} collective-permute-done((bf16[128,2048]{1,0:T(8,128)(2,1)}, bf16[128,2048]{1,0:T(8,128)(2,1)S(1)}, u32[]{:S(2)}, u32[]{:S(2)}) %collective-permute-start.9) | collective-permute-done | bytes 524320 | tf_op jit(solution)/shard_map/ppermute | solution.py:36
  194.0 18.9 %collective-permute-done.10 = bf16[128,2048]{1,0:T(8,128)(2,1)S(1)} collective-permute-done((bf16[128,2048]{1,0:T(8,128)(2,1)S(1)}, bf16[128,2048]{1,0:T(8,128)(2,1)S(1)}, u32[]{:S(2)}, u32[]{:S(2)}) %collective-permute-start.10) | collective-permute-done | bytes 524320 | tf_op jit(solution)/shard_map/ppermute | solution.py:36
  212.9 2.6 pad_maximum_fusion.1
  215.5 3.8 %gather_fusion.2 = bf16[4,128,2048]{2,1,0:T(8,128)(2,1)} fusion(bf16[4,128,2048]{2,1,0:T(8,128)(2,1)} %pad_maximum_fusion.1, s32[1024]{0:T(1024)} %pad_clamp_fusion), kind=kCustom, calls=%fused_computation.2 | custom fusion | bytes 4194320 | tf_op jit(solution)/shard_map/gather | solution.py:46
  219.3 5.5 %fusion.12 = f32[512,768]{1,0:T(8,128)} fusion(bf16[512,2048]{1,0:T(8,128)(2,1)} %bitcast.144, bf16[1,2048,768]{2,1,0:T(8,128)(2,1)} %param.27), kind=kOutput, calls=%fused_computation.16 | convolution fusion | flops 1610612736 | bytes 6815744 | tf_op jit(solution)/shard_map/dot_general | solution.py:69
  224.8 8.3 %fusion.21 = bf16[512,2048]{1,0:T(8,128)(2,1)} fusion(bf16[1,768,2048]{2,1,0:T(8,128)(2,1)S(1)} %copy-done, f32[512,768]{1,0:T(8,128)} %fusion.12, bf16[512,2048]{1,0:T(8,128)(2,1)} %bitcast.145, bf16[1,2048,768]{2,1,0:T(8,128)(2,1)} %param.28), kind=kOutput, calls=%fused_computation.23 | convolution fusion | flops 3224633344 | bytes 12058624 | tf_op jit(solution)/shard_map/dot_general | solution.py:69
  233.1 1.1 reshape.309
  234.2 35.9 %all_to_all.35 = bf16[16,4,2048]{2,1,0:T(4,128)(2,1)} all-to-all(bf16[16,4,2048]{2,1,0:T(4,128)(2,1)S(1)} %reshape.309), channel_id=1, replica_groups=mesh['grp'=2,'sp_0'=16,'sp_1'=2,'tp'=4] {'sp_0'}, dimensions={0} | all-to-all | bytes 524288 | tf_op jit(solution)/shard_map/all_to_all | solution.py:174
  270.1 33.9 %all_to_all.36 = bf16[16,8,2048]{2,1,0:T(8,128)(2,1)} all-to-all(bf16[16,8,2048]{2,1,0:T(8,128)(2,1)} %bitcast.150), channel_id=1, replica_groups=mesh['grp'=2,'sp_0'=16,'sp_1'=2,'tp'=4] {'sp_0'}, dimensions={0} | all-to-all | bytes 1048576 | tf_op jit(solution)/shard_map/all_to_all | solution.py:174
  304.1 12.3 %all-to-all-start.6 = ((bf16[16,8,2048]{2,1,0:T(8,128)(2,1)}), bf16[16,8,2048]{2,1,0:T(8,128)(2,1)}, u32[]{:S(2)}, u32[]{:S(2)}) async-start(bf16[16,8,2048]{2,1,0:T(8,128)(2,1)} %bitcast.151), calls=%async_computation.9 | async-start | bytes 1048576 | tf_op jit(solution)/shard_map/all_to_all | solution.py:174
  318.2 2.6 fusion.109
  320.8 1.8 fusion.64
  322.5 1.8 fusion.66
  324.3 15.0 %all-to-all-done.6 = bf16[16,8,2048]{2,1,0:T(8,128)(2,1)} async-done(((bf16[16,8,2048]{2,1,0:T(8,128)(2,1)}), bf16[16,8,2048]{2,1,0:T(8,128)(2,1)}, u32[]{:S(2)}, u32[]{:S(2)}) %all-to-all-start.6) | async-done | bytes 524320 | tf_op jit(solution)/shard_map/all_to_all | solution.py:174
  339.3 1.6 fusion.60
  341.0 1.5 fusion.62
  342.5 2.5 fusion.27
  345.1 7.0 %collective-permute-start.12 = (f32[128,2048]{1,0:T(8,128)S(1)}, f32[128,2048]{1,0:T(8,128)S(1)}, u32[]{:S(2)}, u32[]{:S(2)}) collective-permute-start(f32[128,2048]{1,0:T(8,128)S(1)} %slice.77), channel_id=1, source_target_pairs={{0,4},{4,0},{1,5},{5,1},{2,6},{6,2},{3,7},{7,3},{8,12},{12,8},{9,1... | collective-permute-start | bytes 3145736 | tf_op jit(solution)/shard_map/ppermute | solution.py:59
  352.1 2.3 collective-permute-done.12
  (115 shorter events, 15.8 us)
Async XLA Ops:
  6.5 134.4 %copy-start = (bf16[1,768,2048]{2,1,0:T(8,128)(2,1)S(1)}, bf16[1,768,2048]{2,1,0:T(8,128)(2,1)}, u32[]{:S(2)}) copy-start(bf16[1,768,2048]{2,1,0:T(8,128)(2,1)} %param.29) | copy-start | bytes 9437188
  8.9 22.4 %collective-permute-start = (f32[4,384]{1,0:T(4,128)S(1)}, f32[4,384]{1,0:T(4,128)S(1)}, u32[]{:S(2)}, u32[]{:S(2)}) collective-permute-start(f32[4,384]{1,0:T(4,128)S(1)} %pad_maximum_fusion.8), channel_id=1, source_target_pairs={{0,4},{4,8},{8,12},{12,16},{16,20},{20,24},{24,28},{28,32},{32,36}... | collective-permute-start | bytes 18440 | tf_op jit(solution)/shard_map/ppermute | solution.py:55
  36.6 4.7 %copy-start.19 = (s32[128,2]{0,1:T(2,128)S(1)}, s32[128,2]{0,1:T(2,128)}, u32[]{:S(2)}) copy-start(s32[128,2]{0,1:T(2,128)} %param.25) | copy-start | bytes 3076
  36.6 4.7 %copy-start.20 = (f32[128,2]{0,1:T(2,128)S(1)}, f32[128,2]{0,1:T(2,128)}, u32[]{:S(2)}) copy-start(f32[128,2]{0,1:T(2,128)} %param.26) | copy-start | bytes 3076
  36.6 30.9 %all-to-all-start = ((bf16[4,128,2048]{2,1,0:T(8,128)(2,1)}), bf16[4,128,2048]{2,1,0:T(8,128)(2,1)}, u32[]{:S(2)}, u32[]{:S(2)}) async-start(bf16[4,128,2048]{2,1,0:T(8,128)(2,1)} %bitcast.143), calls=%async_computation | async-start | bytes 4194304 | tf_op jit(solution)/shard_map/all_to_all | solution.py:124
  41.3 1.3 collective-permute-start.1
  41.6 30.5 %copy-start.17 = (pred[2,2]{1,0:T(4,128)(4,1)}, pred[2,2]{1,0:T(4,128)(4,1)S(1)}, u32[]{:S(2)}) copy-start(pred[2,2]{1,0:T(4,128)(4,1)S(1)} %iota_compare_fusion.1) | copy-start | bytes 16
  67.5 2.2 copy-start.3
  69.7 0.7 copy-start.13
  69.7 0.7 copy-start.14
  70.7 2.7 copy-start.5
  70.7 2.7 collective-permute-start.2
  72.1 1.3 copy-start.10
  73.4 0.8 copy-start.21
  75.3 20.4 %all-to-all-start.1 = ((bf16[16,4,2048]{2,1,0:T(4,128)(2,1)}), bf16[16,4,2048]{2,1,0:T(4,128)(2,1)S(1)}, u32[]{:S(2)}, u32[]{:S(2)}) async-start(bf16[16,4,2048]{2,1,0:T(4,128)(2,1)} %reshape.304), calls=%async_computation.1 | async-start | bytes 524288 | tf_op jit(solution)/shard_map/all_to_all | solution.py:159
  81.9 4.2 %copy-start.6 = (bf16[128,2048]{1,0:T(8,128)(2,1)S(1)}, bf16[128,2048]{1,0:T(8,128)(2,1)}, u32[]{:S(2)}) copy-start(bf16[128,2048]{1,0:T(8,128)(2,1)} %copy-done.5) | copy-start | bytes 1572868
  81.9 4.2 %copy-start.22 = (bf16[128,2048]{1,0:T(8,128)(2,1)S(1)}, bf16[128,2048]{1,0:T(8,128)(2,1)}, u32[]{:S(2)}) copy-start(bf16[128,2048]{1,0:T(8,128)(2,1)} %copy-done.21) | copy-start | bytes 1572868
  95.7 33.3 %all-to-all-start.3 = ((bf16[16,8,2048]{2,1,0:T(8,128)(2,1)}), bf16[16,8,2048]{2,1,0:T(8,128)(2,1)}, u32[]{:S(2)}, u32[]{:S(2)}) async-start(bf16[16,8,2048]{2,1,0:T(8,128)(2,1)} %fusion.31), calls=%async_computation.4 | async-start | bytes 1048576 | tf_op jit(solution)/shard_map/all_to_all | solution.py:159
  106.1 127.0 %reduce-scatter.4.cloned.1.call-start = ((), (), s32[]{:S(2)}) async-start(), calls=%async_computation.10 | async-start | bytes 1310720 | tf_op jit(solution)/shard_map/reduce_scatter | solution.py:170
  106.9 8.5 %collective-permute-start.3 = (bf16[64,2048]{1,0:T(8,128)(2,1)}, bf16[64,2048]{1,0:T(8,128)(2,1)}, u32[]{:S(2)}, u32[]{:S(2)}) collective-permute-start(bf16[64,2048]{1,0:T(8,128)(2,1)} %reshape.307), channel_id=1, source_target_pairs={{0,1},{1,2},{2,3},{3,0},{4,5},{5,6},{6,7},{7,4},{8,9},{9,10},{10,1... | collective-permute-start | bytes 786440 | tf_op jit(solution)/shard_map/ppermute | solution.py:36
  107.4 22.0 %collective-permute-start.5 = (bf16[64,2048]{1,0:T(8,128)(2,1)}, bf16[64,2048]{1,0:T(8,128)(2,1)}, u32[]{:S(2)}, u32[]{:S(2)}) collective-permute-start(bf16[64,2048]{1,0:T(8,128)(2,1)} %reshape.307), channel_id=1, source_target_pairs={{1,0},{2,1},{3,2},{0,3},{5,4},{6,5},{7,6},{4,7},{9,8},{10,9},{11,1... | collective-permute-start | bytes 786440 | tf_op jit(solution)/shard_map/ppermute | solution.py:40
  115.4 14.0 %collective-permute-start.4 = (bf16[64,2048]{1,0:T(8,128)(2,1)}, bf16[64,2048]{1,0:T(8,128)(2,1)}, u32[]{:S(2)}, u32[]{:S(2)}) collective-permute-start(bf16[64,2048]{1,0:T(8,128)(2,1)} %collective-permute-done.3), channel_id=1, source_target_pairs={{0,1},{1,2},{2,3},{3,0},{4,5},{5,6},{6,7},{7,4},{8,9},{9,10},{10,1... | collective-permute-start | bytes 786440 | tf_op jit(solution)/shard_map/ppermute | solution.py:36
  129.0 12.0 %collective-permute-start.6 = (bf16[128,2048]{1,0:T(8,128)(2,1)}, bf16[128,2048]{1,0:T(8,128)(2,1)}, u32[]{:S(2)}, u32[]{:S(2)}) collective-permute-start(bf16[128,2048]{1,0:T(8,128)(2,1)} %bitcast.18), channel_id=1, source_target_pairs={{0,1},{1,2},{2,3},{3,0},{4,5},{5,6},{6,7},{7,4},{8,9},{9,10},{10,1... | collective-permute-start | bytes 1572872 | tf_op jit(solution)/shard_map/ppermute | solution.py:36
  138.8 23.1 %collective-permute-start.8 = (bf16[128,2048]{1,0:T(8,128)(2,1)}, bf16[128,2048]{1,0:T(8,128)(2,1)}, u32[]{:S(2)}, u32[]{:S(2)}) collective-permute-start(bf16[128,2048]{1,0:T(8,128)(2,1)} %bitcast.18), channel_id=1, source_target_pairs={{1,0},{2,1},{3,2},{0,3},{5,4},{6,5},{7,6},{4,7},{9,8},{10,9},{11,1... | collective-permute-start | bytes 1572872 | tf_op jit(solution)/shard_map/ppermute | solution.py:40
  141.0 20.9 %collective-permute-start.7 = (bf16[128,2048]{1,0:T(8,128)(2,1)}, bf16[128,2048]{1,0:T(8,128)(2,1)}, u32[]{:S(2)}, u32[]{:S(2)}) collective-permute-start(bf16[128,2048]{1,0:T(8,128)(2,1)} %collective-permute-done.6), channel_id=1, source_target_pairs={{0,1},{1,2},{2,3},{3,0},{4,5},{5,6},{6,7},{7,4},{8,9},{9,10},{10,1... | collective-permute-start | bytes 1572872 | tf_op jit(solution)/shard_map/ppermute | solution.py:36
  146.6 37.9 %all-to-all-start.5 = ((bf16[16,8,2048]{2,1,0:T(8,128)(2,1)}), bf16[16,8,2048]{2,1,0:T(8,128)(2,1)}, u32[]{:S(2)}, u32[]{:S(2)}) async-start(bf16[16,8,2048]{2,1,0:T(8,128)(2,1)} %fusion.32), calls=%async_computation.7 | async-start | bytes 1048576 | tf_op jit(solution)/shard_map/all_to_all | solution.py:159
  161.8 108.3 %reduce-scatter.6.cloned.1.call-start = ((), (), s32[]{:S(2)}) async-start(), calls=%async_computation.11 | async-start | bytes 2621440 | tf_op jit(solution)/shard_map/reduce_scatter | solution.py:170
  182.6 121.5 %reduce-scatter.8.cloned.1.call-start = ((), (), s32[]{:S(2)}) async-start(), calls=%async_computation.12 | async-start | bytes 2621440 | tf_op jit(solution)/shard_map/reduce_scatter | solution.py:170
  184.5 9.5 %collective-permute-start.9 = (bf16[128,2048]{1,0:T(8,128)(2,1)}, bf16[128,2048]{1,0:T(8,128)(2,1)S(1)}, u32[]{:S(2)}, u32[]{:S(2)}) collective-permute-start(bf16[128,2048]{1,0:T(8,128)(2,1)} %bitcast.26), channel_id=1, source_target_pairs={{0,1},{1,2},{2,3},{3,0},{4,5},{5,6},{6,7},{7,4},{8,9},{9,10},{10,1... | collective-permute-start | bytes 1572872 | tf_op jit(solution)/shard_map/ppermute | solution.py:36
  184.5 9.5 %collective-permute-start.11 = (bf16[128,2048]{1,0:T(8,128)(2,1)}, bf16[128,2048]{1,0:T(8,128)(2,1)S(1)}, u32[]{:S(2)}, u32[]{:S(2)}) collective-permute-start(bf16[128,2048]{1,0:T(8,128)(2,1)} %bitcast.26), channel_id=1, source_target_pairs={{1,0},{2,1},{3,2},{0,3},{5,4},{6,5},{7,6},{4,7},{9,8},{10,9},{11,1... | collective-permute-start | bytes 1572872 | tf_op jit(solution)/shard_map/ppermute | solution.py:40
  194.0 18.9 %collective-permute-start.10 = (bf16[128,2048]{1,0:T(8,128)(2,1)S(1)}, bf16[128,2048]{1,0:T(8,128)(2,1)S(1)}, u32[]{:S(2)}, u32[]{:S(2)}) collective-permute-start(bf16[128,2048]{1,0:T(8,128)(2,1)S(1)} %collective-permute-done.9), channel_id=1, source_target_pairs={{0,1},{1,2},{2,3},{3,0},{4,5},{5,6},{6,7},{7,4},{8,9},{9,10},{10,1... | collective-permute-start | bytes 1572872 | tf_op jit(solution)/shard_map/ppermute | solution.py:36
  270.1 46.3 %copy-start.11 = (pred[16,2,2,128]{3,2,1,0:T(4,128)(4,1)S(1)}, pred[16,2,2,128]{3,2,1,0:T(4,128)(4,1)}, u32[]{:S(2)}) copy-start(pred[16,2,2,128]{3,2,1,0:T(4,128)(4,1)} %copy-done.10) | copy-start | bytes 24580
  270.1 46.3 %copy-start.18 = (pred[2,2]{1,0:T(4,128)(4,1)S(1)}, pred[2,2]{1,0:T(4,128)(4,1)}, u32[]{:S(2)}) copy-start(pred[2,2]{1,0:T(4,128)(4,1)} %copy-done.17) | copy-start | bytes 16
  304.1 35.3 %all-to-all-start.6 = ((bf16[16,8,2048]{2,1,0:T(8,128)(2,1)}), bf16[16,8,2048]{2,1,0:T(8,128)(2,1)}, u32[]{:S(2)}, u32[]{:S(2)}) async-start(bf16[16,8,2048]{2,1,0:T(8,128)(2,1)} %bitcast.151), calls=%async_computation.9 | async-start | bytes 1048576 | tf_op jit(solution)/shard_map/all_to_all | solution.py:174
  318.1 2.6 copy-start.4
  318.2 2.6 copy-start.9
  318.2 4.4 %copy-start.8 = (bf16[16,2,4,2,128]{4,3,2,1,0:T(2,128)(2,1)S(1)}, bf16[16,2,4,2,128]{4,3,2,1,0:T(2,128)(2,1)}, u32[]{:S(2)}) copy-start(bf16[16,2,4,2,128]{4,3,2,1,0:T(2,128)(2,1)} %get-tuple-element.21) | copy-start | bytes 196612
  339.3 3.2 copy-start.1
  339.3 3.2 copy-start.2
  339.3 3.2 copy-start.12
  345.0 9.4 %copy-start.7 = (bf16[128,2048]{1,0:T(8,128)(2,1)S(1)}, bf16[128,2048]{1,0:T(8,128)(2,1)}, u32[]{:S(2)}) copy-start(bf16[128,2048]{1,0:T(8,128)(2,1)} %copy-done.5) | copy-start | bytes 1572868
  345.1 9.9 %copy-start.15 = (f32[2048]{0:T(1024)S(1)}, f32[2048]{0:T(1024)}, u32[]{:S(2)}) copy-start(f32[2048]{0:T(1024)} %param.31) | copy-start | bytes 24580
  345.1 9.9 %copy-start.16 = (f32[2048]{0:T(1024)S(1)}, f32[2048]{0:T(1024)}, u32[]{:S(2)}) copy-start(f32[2048]{0:T(1024)} %param.30) | copy-start | bytes 24580
  345.1 9.3 %collective-permute-start.12 = (f32[128,2048]{1,0:T(8,128)S(1)}, f32[128,2048]{1,0:T(8,128)S(1)}, u32[]{:S(2)}, u32[]{:S(2)}) collective-permute-start(f32[128,2048]{1,0:T(8,128)S(1)} %slice.77), channel_id=1, source_target_pairs={{0,4},{4,0},{1,5},{5,1},{2,6},{6,2},{3,7},{7,3},{8,12},{12,8},{9,1... | collective-permute-start | bytes 3145736 | tf_op jit(solution)/shard_map/ppermute | solution.py:59
Sparse Core Ops, SparseCore 0:
  146.7 34.3 reduce-scatter.3
  183.7 47.1 reduce-scatter.5
  233.4 48.4 reduce-scatter.7
